TPU v7x, 32 devices: a whole 2x2x4 slice. The times are simulated.
32 devices in a mesh: ep: 8 (over z, y), tp: 4 (over x, core).
Axes of the slice: x: 2, y: 2, z: 4, core: 2. Of those that a mesh axis runs over, the one named last changes fastest.
Arguments:
- hidden_in: bfloat16 [384, 2048], P('ep'), may hold values from -6 to 6
- carried_state: float32 [384, 4, 128, 256], P('ep', 'tp'), may hold values from -6 to 6
- input_gain: bfloat16 [2048], replicated, may hold values from 0.099609375 to 1.8984375
- query_weight: bfloat16 [2048, 512], P(None, 'tp'), may hold values from -0.125 to 0.125
- key_weight: bfloat16 [2048, 512], P(None, 'tp'), may hold values from -0.125 to 0.125
- value_weight: bfloat16 [2048, 1024], P(None, 'tp'), may hold values from -0.125 to 0.125
- outgate_weight: bfloat16 [2048, 1024], P(None, 'tp'), may hold values from -0.125 to 0.125
- decay_weight: bfloat16 [2048, 512], P(None, 'tp'), may hold values from -0.5 to 0.5
- decay_shift: float32 [384, 512], P('ep', 'tp'), may hold values from -0.7 to 0
- head_gain: bfloat16 [4, 256], P('tp'), may hold values from 0.099609375 to 1.8984375
- output_weight: bfloat16 [1024, 2048], P('tp'), may hold values from -0.1875 to 0.1875
- channel_gain: bfloat16 [2048], replicated, may hold values from 0.099609375 to 1.8984375
- branch_gate: bfloat16 [2048], replicated, may hold values from -0.125 to 0.125
- routes: int32 [384, 2], P('ep'), may hold values from 0 to 7, all different within a row; in each aligned block of 48 rows (0 to 47, 48 to 95, ...) at most 14 rows name the same one
- route_weights: float32 [384, 2], P('ep'), may hold values from 0.1 to 1
- expert_gate: bfloat16 [8, 2048, 3072], P('ep', None, 'tp'), may hold values from -0.125 to 0.125
- expert_up: bfloat16 [8, 2048, 3072], P('ep', None, 'tp'), may hold values from -0.125 to 0.125
- expert_down: bfloat16 [8, 3072, 2048], P('ep', 'tp'), may hold values from -0.109375 to 0.109375
- dense_gate: bfloat16 [2048, 4096], P('tp', 'ep'), may hold values from -0.125 to 0.125
- dense_up: bfloat16 [2048, 4096], P('tp', 'ep'), may hold values from -0.125 to 0.125
- dense_down: bfloat16 [4096, 2048], P('ep', 'tp'), may hold values from -0.09375 to 0.09375
Outputs:
- mixed: bfloat16 [384, 2048], P('ep', 'tp')
- new_state: float32 [384, 4, 128, 256], P('ep', 'tp')
Inputs may be any that keep to these rules, and one draw needn't show every extreme that they name: `routes`: each row names 2 different experts. Among the rows of one index of ep no expert is named more than 14 times, and in every draw some expert is named exactly 14 times by the rows of some index.
All inputs are finite; a program needn't handle non-finite values.
Results may differ from a plain program's by a relative error of at most 0.02.
Values may be sent and summed in bfloat16 or wider, within the bound.
No kernel may reach another device: no remote copies, remote signals or barrier semaphores. Data moves between devices by JAX's collectives and lax.ppermute only.
A program may use at most 128 MiB of HBM per device.

v0:
```python
import jax
import jax.numpy as jnp
from jax import lax
from jax.sharding import PartitionSpec as P

EPSILON = 1e-06
TAU_DECAY = 16.0


def rms_factor(values):
    return lax.rsqrt(jnp.mean(values * values, axis=-1, keepdims=True) + EPSILON)


def rounded(values):
    return lax.optimization_barrier(values.astype(jnp.bfloat16)).astype(jnp.float32)


def matmul(left, right):
    return jnp.dot(left, right, preferred_element_type=jnp.float32)


def unit_totals(paired):
    return lax.psum(paired.astype(jnp.bfloat16), "tp").astype(jnp.float32)


def body(
    hidden_in,
    carried_state,
    input_gain,
    query_weight,
    key_weight,
    value_weight,
    outgate_weight,
    decay_weight,
    decay_shift,
    head_gain,
    output_weight,
    channel_gain,
    branch_gate,
    routes,
    route_weights,
    expert_gate,
    expert_up,
    expert_down,
    dense_gate,
    dense_up,
    dense_down,
):
    tokens_here, width = hidden_in.shape
    heads_here, key_dim, value_dim = carried_state.shape[1:]
    quarter = width // lax.axis_size("tp")
    lane_start = lax.axis_index("tp") * quarter
    inputs = hidden_in.astype(jnp.float32)
    normed = (inputs * rms_factor(inputs) * input_gain.astype(jnp.float32)).astype(jnp.bfloat16)
    query = matmul(normed, query_weight).astype(jnp.bfloat16)
    key_rows = matmul(normed, key_weight).astype(jnp.bfloat16)
    value_rows = matmul(normed, value_weight).astype(jnp.bfloat16)
    outgate = matmul(normed, outgate_weight).astype(jnp.bfloat16)
    decay = jnp.exp(jax.nn.log_sigmoid(matmul(normed, decay_weight)) / TAU_DECAY + decay_shift)
    decay = decay.reshape(tokens_here, heads_here, key_dim)
    query_scaled = query.astype(jnp.float32).reshape(
        tokens_here, heads_here, key_dim
    ) * key_dim ** (-0.5)
    key_vals = key_rows.astype(jnp.float32).reshape(tokens_here, heads_here, key_dim)
    value_vals = value_rows.astype(jnp.float32).reshape(tokens_here, heads_here, value_dim)
    new_state = decay[..., None] * carried_state + key_vals[..., None] * value_vals[:, :, None, :]
    readout = jnp.einsum("bhk,bhkv->bhv", query_scaled, new_state, precision=lax.Precision.HIGHEST)
    gate_vals = jax.nn.silu(outgate.astype(jnp.float32).reshape(tokens_here, heads_here, value_dim))
    gated = (readout * rms_factor(readout) * head_gain.astype(jnp.float32) * gate_vals).astype(
        jnp.bfloat16
    )
    partial_out = rounded(matmul(gated.reshape(tokens_here, heads_here * value_dim), output_weight))
    own_gain = lax.dynamic_slice_in_dim(channel_gain.astype(jnp.float32), lane_start, quarter, 0)
    own_branch = lax.dynamic_slice_in_dim(branch_gate.astype(jnp.float32), lane_start, quarter, 0)
    attended_own = lax.psum_scatter(
        partial_out.astype(jnp.bfloat16), "tp", scatter_dimension=1, tiled=True
    ).astype(jnp.float32)
    middle_own = rounded(lax.dynamic_slice_in_dim(inputs, lane_start, quarter, 1) + attended_own)
    total_squares, gate_inner = lax.psum(
        (
            jnp.sum(middle_own * middle_own, axis=-1),
            jnp.sum(middle_own * own_gain * own_branch, axis=-1),
        ),
        "tp",
    )
    factor = lax.rsqrt(total_squares / width + EPSILON)
    branch = jax.nn.sigmoid(gate_inner * factor)
    ffn_own = (middle_own * factor[:, None] * own_gain).astype(jnp.bfloat16)
    expert_count = lax.axis_size("ep")
    topk = routes.shape[1]
    capacity = tokens_here * topk // expert_count + 2
    chosen = (
        routes[:, :, None] == jnp.arange(expert_count, dtype=jnp.int32)[None, None, :]
    ).astype(jnp.int32)
    chosen_flat = chosen.reshape(tokens_here * topk, expert_count)
    earlier = jnp.cumsum(chosen_flat, axis=0) - chosen_flat
    slot_index = jnp.sum(earlier * chosen_flat, axis=1).reshape(tokens_here, topk)
    position = routes * capacity + slot_index
    slot_table = jnp.arange(expert_count * capacity, dtype=jnp.int32)
    selector = jnp.sum(
        (slot_table[:, None, None] == position[None, :, :]).astype(jnp.bfloat16), axis=2
    )
    send_width = ffn_own.shape[1]
    outgoing = (
        matmul(selector, ffn_own).astype(jnp.bfloat16).reshape(expert_count, capacity, send_width)
    )
    full_rows = lax.all_gather(
        lax.all_to_all(outgoing, "ep", split_axis=0, concat_axis=0, tiled=True),
        "tp",
        axis=2,
        tiled=True,
    )
    sources = full_rows.shape[0]
    items = full_rows.shape[1]
    flat_rows = full_rows.reshape(sources * items, width)
    gate_part = matmul(flat_rows, expert_gate[0])
    up_part = matmul(flat_rows, expert_up[0])
    hidden = (jax.nn.silu(gate_part) * up_part).astype(jnp.bfloat16)
    block_out = rounded(matmul(hidden, expert_down[0]))
    summed = lax.psum_scatter(
        block_out.astype(jnp.bfloat16), "tp", scatter_dimension=1, tiled=True
    ).astype(jnp.float32)
    returned = lax.all_to_all(
        summed.reshape(sources, items, quarter).astype(jnp.bfloat16),
        "ep",
        split_axis=0,
        concat_axis=0,
        tiled=True,
    ).astype(jnp.float32)
    flat_back = returned.reshape(expert_count * capacity, quarter)
    picked = jnp.take(flat_back, position.reshape(-1), axis=0).reshape(tokens_here, topk, quarter)
    routed_own = jnp.sum(picked * route_weights[:, :, None], axis=1)
    piece = lax.all_gather(ffn_own, "ep", axis=0, tiled=True)
    paired = unit_totals(
        jnp.concatenate([matmul(piece, dense_gate), matmul(piece, dense_up)], axis=1)
    )
    units = dense_gate.shape[1]
    dense_hidden = (jax.nn.silu(paired[:, :units]) * paired[:, units:]).astype(jnp.bfloat16)
    dense_own = lax.psum_scatter(
        matmul(dense_hidden, dense_down).astype(jnp.bfloat16), "ep", scatter_dimension=0, tiled=True
    ).astype(jnp.float32)
    mixed = (middle_own + branch[:, None] * dense_own + routed_own).astype(jnp.bfloat16)
    return (mixed, new_state)


def solution(mesh):
    in_specs = (
        P("ep", None),
        P("ep", "tp", None, None),
        P(),
        P(None, "tp"),
        P(None, "tp"),
        P(None, "tp"),
        P(None, "tp"),
        P(None, "tp"),
        P("ep", "tp"),
        P("tp", None),
        P("tp", None),
        P(),
        P(),
        P("ep", None),
        P("ep", None),
        P("ep", None, "tp"),
        P("ep", None, "tp"),
        P("ep", "tp", None),
        P("tp", "ep"),
        P("tp", "ep"),
        P("ep", "tp"),
    )
    out_specs = (P("ep", "tp"), P("ep", "tp", None, None))
    return jax.shard_map(body, mesh=mesh, in_specs=in_specs, out_specs=out_specs, check_vma=False)
```

profile of v0, /device:TPU:0, one launch (start us, length us, event | category | flops | bytes accessed | tf_op | source)
XLA Modules:
  0.0 232.2 jit_solution(6923637545601130041)
XLA Ops:
  7.2 0.0 reduce-scatter.4.cloned.1.call-start
  7.2 0.8 convert_element_type.104
  8.1 1.1 multiply_reduce_fusion
  9.2 1.7 fusion.18
  10.9 1.4 fusion.19
  12.3 1.4 fusion.21
  13.7 1.4 fusion.50
  15.1 4.5 %multiply_add_fusion = f32[48,1,128,256]{3,2,1,0:T(8,128)S(1)} fusion(f32[48,1,128,256]{3,2,1,0:T(8,128)} %param.22, f32[48,256]{1,0:T(8,128)S(1)} %fusion.18, f32[48,128]{1,0:T(8,128)S(1)} %fusion.19, f32[48,128]{1,0:T(8,128)S(1)} %fusion.50), kind=kLoop, calls=%fused_computation.3 | loop fusion | flops 4718592 | bytes 12681216 | tf_op jit(solution)/shard_map/add | solution.py:66
  19.7 3.1 %fusion = f32[48,1,256]{2,1,0:T(1,128)S(1)} fusion(f32[48,128,1]{1,2,0:T(1,128)S(1)} %bitcast.55, f32[48,1,128,256]{3,2,1,0:T(8,128)S(1)} %multiply_add_fusion), kind=kOutput, calls=%fused_computation.1 | convolution fusion | flops 18874368 | bytes 6365184 | tf_op jit(solution)/shard_map/bhk,bhkv->bhv/dot_general | solution.py:67
  22.7 0.1 fusion.39
  22.9 3.0 %convolution_convert_fusion = bf16[48,2048]{1,0:T(8,128)(2,1)} fusion(bf16[256,2048]{1,0:T(8,128)(2,1)} %param.31, bf16[2048,256]{1,0:T(8,128)(2,1)} %param.27, f32[48,1,256]{2,1,0:T(1,128)S(1)} %fusion, f32[256]{0:T(256)S(1)} %bitcast.56, f32[48]{0:T(128)S(1)} %add_rsqrt_fusion.1, f32[2048]{0:T(1024)S(1)} %convert_element_type.104, ...), kind=kOutput, calls=%fused_computation.11 | convolution fusion | flops 101277696 | bytes 2549120 | tf_op jit(solution)/shard_map/dot_general | solution.py:19
  25.9 0.0 reduce-scatter.4.cloned.1.call-update
  26.0 0.1 copy.36
  26.0 0.1 eq.29
  26.2 0.1 fusion.43
  26.3 0.1 reduce_window_sum.11
  26.4 0.2 select_reduce_fusion
  26.6 0.8 dynamic-slice_convert_fusion
  27.4 0.8 convert_element_type.103
  28.1 0.1 reshape.135
  28.2 0.1 copy.37
  28.3 0.5 compare_and_fusion
  28.9 0.1 fusion.46
  29.0 19.7 %reduce-scatter.4.cloned.1.call-done = bf16[48,512]{1,0:T(8,128)(2,1)} async-done(((bf16[48,2048]{1,0:T(8,128)(2,1)}), bf16[48,512]{1,0:T(8,128)(2,1)}) %reduce-scatter.4.cloned.1.call-update) | async-done | bytes 49168 | tf_op jit(solution)/shard_map/reduce_scatter | solution.py:75
  48.6 0.9 add_convert_fusion
  49.6 0.1 fusion.33
  49.7 5.8 %all-reduce = (f32[48]{0:T(128)S(1)}, f32[48]{0:T(128)S(1)}) all-reduce(f32[48]{0:T(128)S(1)} %get-tuple-element.3, f32[48]{0:T(128)S(1)} %get-tuple-element.2), channel_id=1, replica_groups=mesh['ep'=8,'tp'=4] {'tp'}, use_global_device_ids=true, to_apply=%region_6.7 | all-reduce | flops 96 | bytes 768 | tf_op jit(solution)/shard_map/psum | solution.py:79
  55.5 0.6 add_divide_fusion
  56.0 0.1 fusion.36
  56.1 31.5 %all_gather.6 = bf16[384,512]{1,0:T(8,128)(2,1)S(1)} all-gather(bf16[48,512]{1,0:T(8,128)(2,1)S(1)} %fusion.36), channel_id=1, replica_groups=mesh['ep'=8,'tp'=4] {'ep'}, dimensions={0}, use_global_device_ids=true | all-gather | bytes 442368 | tf_op jit(solution)/shard_map/all_gather | solution.py:133
  87.6 0.8 convolution_convert_fusion.4
  88.5 1.6 reshape.136
  90.1 5.3 %all-to-all-start = ((bf16[8,14,512]{2,1,0:T(8,128)(2,1)}), bf16[8,14,512]{2,1,0:T(8,128)(2,1)}, u32[]{:S(2)}, u32[]{:S(2)}) async-start(bf16[8,14,512]{2,1,0:T(8,128)(2,1)} %reshape.136), calls=%async_computation.2 | async-start | bytes 262144 | tf_op jit(solution)/shard_map/all_to_all | solution.py:108
  95.4 0.0 all-reduce.3.cloned.1.call-start
  95.4 1.4 convolution_convert_fusion.2
  96.8 1.4 convolution_convert_fusion.3
  98.3 1.0 pad_maximum_fusion
  99.3 0.0 all-reduce.3.cloned.1.call-update
  99.3 0.0 reduce-scatter.8.cloned.1.call-start
  99.3 3.5 %all-to-all-done = bf16[8,14,512]{2,1,0:T(8,128)(2,1)} async-done(((bf16[8,14,512]{2,1,0:T(8,128)(2,1)}), bf16[8,14,512]{2,1,0:T(8,128)(2,1)}, u32[]{:S(2)}, u32[]{:S(2)}) %all-to-all-start) | async-done | bytes 114720 | tf_op jit(solution)/shard_map/all_to_all | solution.py:108
  102.8 9.9 %all_gather.7 = bf16[8,14,2048]{2,1,0:T(8,128)(2,1)} all-gather(bf16[8,14,512]{2,1,0:T(8,128)(2,1)} %all-to-all-done), channel_id=1, replica_groups=mesh['ep'=8,'tp'=4] {'tp'}, dimensions={2}, use_global_device_ids=true | all-gather | bytes 573440 | tf_op jit(solution)/shard_map/all_gather | solution.py:107
  112.8 1.9 reshape.137
  114.7 2.6 %fusion.6 = f32[112,768]{1,0:T(8,128)S(1)} fusion(bf16[112,2048]{1,0:T(8,128)(2,1)} %reshape.137, bf16[1,2048,768]{2,1,0:T(8,128)(2,1)} %param.36), kind=kOutput, calls=%fused_computation.8 | convolution fusion | flops 352321536 | bytes 3948544 | tf_op jit(solution)/shard_map/dot_general | solution.py:19
  117.4 4.1 %fusion.8 = bf16[112,2048]{1,0:T(8,128)(2,1)} fusion(bf16[1,768,2048]{2,1,0:T(8,128)(2,1)S(1)} %copy-done, bf16[112,2048]{1,0:T(8,128)(2,1)} %reshape.137, bf16[1,2048,768]{2,1,0:T(8,128)(2,1)} %param.37, f32[112,768]{1,0:T(8,128)S(1)} %fusion.6), kind=kOutput, calls=%fused_computation.10 | convolution fusion | flops 705388544 | bytes 7553024 | tf_op jit(solution)/shard_map/dot_general | solution.py:19
  121.5 0.0 reduce-scatter.8.cloned.1.call-update
  121.5 0.0 reduce-scatter.6.cloned.1.call-start
  121.5 13.5 %all-reduce.3.cloned.1.call-done = bf16[384,1024]{1,0:T(8,128)(2,1)} async-done(((bf16[384,1024]{1,0:T(8,128)(2,1)}), bf16[384,1024]{1,0:T(8,128)(2,1)}) %all-reduce.3.cloned.1.call-update) | async-done | bytes 786448 | tf_op jit(solution)/shard_map/psum | solution.py:23
  135.0 1.3 convert_element_type.122
  136.4 2.2 convolution_convert_fusion.1
  138.6 0.0 reduce-scatter.6.cloned.1.call-update
  138.6 0.1 copy.39
  138.7 0.1 reshape.140
  138.8 20.0 %reduce-scatter.8.cloned.1.call-done = bf16[112,512]{1,0:T(8,128)(2,1)} async-done(((bf16[112,2048]{1,0:T(8,128)(2,1)}), bf16[112,512]{1,0:T(8,128)(2,1)}) %reduce-scatter.8.cloned.1.call-update) | async-done | bytes 114704 | tf_op jit(solution)/shard_map/reduce_scatter | solution.py:120
  158.8 1.6 convert_element_type.131
  160.4 5.5 %all-to-all-start.1 = ((bf16[8,14,512]{2,1,0:T(8,128)(2,1)}), bf16[8,14,512]{2,1,0:T(8,128)(2,1)S(1)}, u32[]{:S(2)}, u32[]{:S(2)}) async-start(bf16[8,14,512]{2,1,0:T(8,128)(2,1)} %convert_element_type.131), calls=%async_computation.4 | async-start | bytes 262144 | tf_op jit(solution)/shard_map/all_to_all | solution.py:123
  165.9 0.7 copy.38
  166.6 0.7 copy.40
  167.3 0.6 pad_clamp_fusion
  167.9 5.4 %all-to-all-done.1 = bf16[8,14,512]{2,1,0:T(8,128)(2,1)S(1)} async-done(((bf16[8,14,512]{2,1,0:T(8,128)(2,1)}), bf16[8,14,512]{2,1,0:T(8,128)(2,1)S(1)}, u32[]{:S(2)}, u32[]{:S(2)}) %all-to-all-start.1) | async-done | bytes 114720 | tf_op jit(solution)/shard_map/all_to_all | solution.py:123
  173.3 1.5 gather_fusion
  174.8 1.0 gather.7
  175.8 1.1 multiply_reduce_fusion.1
  176.9 47.2 %reduce-scatter.6.cloned.1.call-done = bf16[48,512]{1,0:T(8,128)(2,1)} async-done(((bf16[384,512]{1,0:T(8,128)(2,1)}), bf16[48,512]{1,0:T(8,128)(2,1)}) %reduce-scatter.6.cloned.1.call-update) | async-done | bytes 49168 | tf_op jit(solution)/shard_map/reduce_scatter | solution.py:139
  224.2 1.5 fusion.38
  (23 shorter events, 0.1 us)
Async XLA Ops:
  7.2 110.2 %copy-start = (bf16[1,768,2048]{2,1,0:T(8,128)(2,1)S(1)}, bf16[1,768,2048]{2,1,0:T(8,128)(2,1)}, u32[]{:S(2)}) copy-start(bf16[1,768,2048]{2,1,0:T(8,128)(2,1)} %param.38) | copy-start | bytes 9437188
  7.2 41.4 %reduce-scatter.4.cloned.1.call-start = ((), (), s32[]{:S(2)}) async-start(), calls=%async_computation.5 | async-start | bytes 245760 | tf_op jit(solution)/shard_map/reduce_scatter | solution.py:75
  19.6 3.1 %copy-start.1 = (f32[48,1,128,256]{3,2,1,0:T(8,128)}, f32[48,1,128,256]{3,2,1,0:T(8,128)S(1)}, u32[]{:S(2)}) copy-start(f32[48,1,128,256]{3,2,1,0:T(8,128)S(1)} %multiply_add_fusion) | copy-start | bytes 18874372
  19.6 3.3 %copy-start.8 = (bf16[1,256]{1,0:T(2,128)(2,1)S(1)}, bf16[1,256]{1,0:T(2,128)(2,1)}, u32[]{:S(2)}) copy-start(bf16[1,256]{1,0:T(2,128)(2,1)} %param.30) | copy-start | bytes 1540
  19.6 3.3 %copy-start.2 = (bf16[48,2048]{1,0:T(8,128)(2,1)S(1)}, bf16[48,2048]{1,0:T(8,128)(2,1)}, u32[]{:S(2)}) copy-start(bf16[48,2048]{1,0:T(8,128)(2,1)} %param.21) | copy-start | bytes 589828
  19.6 6.3 %copy-start.5 = (s32[48,2]{0,1:T(2,128)S(1)}, s32[48,2]{0,1:T(2,128)}, u32[]{:S(2)}) copy-start(s32[48,2]{0,1:T(2,128)} %param.34) | copy-start | bytes 1156
  49.6 6.5 %copy-start.3 = (bf16[48,512]{1,0:T(8,128)(2,1)}, bf16[48,512]{1,0:T(8,128)(2,1)S(1)}, u32[]{:S(2)}) copy-start(bf16[48,512]{1,0:T(8,128)(2,1)S(1)} %add_convert_fusion) | copy-start | bytes 147460
  90.1 12.8 %all-to-all-start = ((bf16[8,14,512]{2,1,0:T(8,128)(2,1)}), bf16[8,14,512]{2,1,0:T(8,128)(2,1)}, u32[]{:S(2)}, u32[]{:S(2)}) async-start(bf16[8,14,512]{2,1,0:T(8,128)(2,1)} %reshape.136), calls=%async_computation.2 | async-start | bytes 262144 | tf_op jit(solution)/shard_map/all_to_all | solution.py:108
  95.4 39.7 %all-reduce.3.cloned.1.call-start = ((), (), s32[]{:S(2)}) async-start(), calls=%async_computation.6 | async-start | bytes 1572864 | tf_op jit(solution)/shard_map/psum | solution.py:23
  99.3 59.5 %reduce-scatter.8.cloned.1.call-start = ((), (), s32[]{:S(2)}) async-start(), calls=%async_computation.8 | async-start | bytes 573440 | tf_op jit(solution)/shard_map/reduce_scatter | solution.py:120
  121.5 102.7 %reduce-scatter.6.cloned.1.call-start = ((), (), s32[]{:S(2)}) async-start(), calls=%async_computation.7 | async-start | bytes 442368 | tf_op jit(solution)/shard_map/reduce_scatter | solution.py:139
  136.4 29.6 %copy-start.6 = (pred[48,2]{0,1:T(4,128)(4,1)S(1)}, pred[48,2]{0,1:T(4,128)(4,1)}, u32[]{:S(2)}) copy-start(pred[48,2]{0,1:T(4,128)(4,1)} %get-tuple-element.6) | copy-start | bytes 292
  136.4 30.2 %copy-start.7 = (f32[48,2]{0,1:T(2,128)S(1)}, f32[48,2]{0,1:T(2,128)}, u32[]{:S(2)}) copy-start(f32[48,2]{0,1:T(2,128)} %param.35) | copy-start | bytes 1156
  138.6 85.6 %copy-start.4 = (bf16[48,512]{1,0:T(8,128)(2,1)S(1)}, bf16[48,512]{1,0:T(8,128)(2,1)}, u32[]{:S(2)}) copy-start(bf16[48,512]{1,0:T(8,128)(2,1)} %copy-done.3) | copy-start | bytes 147460
  160.4 12.9 %all-to-all-start.1 = ((bf16[8,14,512]{2,1,0:T(8,128)(2,1)}), bf16[8,14,512]{2,1,0:T(8,128)(2,1)S(1)}, u32[]{:S(2)}, u32[]{:S(2)}) async-start(bf16[8,14,512]{2,1,0:T(8,128)(2,1)} %convert_element_type.131), calls=%async_computation.4 | async-start | bytes 262144 | tf_op jit(solution)/shard_map/all_to_all | solution.py:123
Sparse Core Ops, SparseCore 0:
  26.1 22.5 reduce-scatter.3
  99.4 35.5 all-reduce.2
  137.6 21.1 reduce-scatter.7
  161.9 62.2 reduce-scatter.5
where the time goes:
time: 233 us; the launch traced here: 232 us
  waiting for transfers between devices  109 us (47%)
  blocking collectives  47.2 us (20%)
  matrix products  24.6 us (11%)
  other arithmetic  16.3 us (7%)
  between operations  14 us (6%)
  starting transfers between devices  11 us (5%)
  local copies, waits for them, and re-layouts  9.71 us (4%)
    reduce_scatter x1, waiting for transfers between devices, body(): lax.psum_scatter(matmul(dense_hidden, dense_down).astype(jnp.bfloat16), '...  47.2 us
    all_gather x1, blocking collectives, body(): piece = lax.all_gather(ffn_own, 'ep', axis=0, tiled=True)  31.5 us
    dot_general x11, matrix products, matmul(): return jnp.dot(left, right, preferred_element_type=jnp.float32)  21.5 us
    reduce_scatter x1, waiting for transfers between devices, body(): lax.psum_scatter(block_out.astype(jnp.bfloat16), 'tp', scatter_dimension=...  20 us
    reduce_scatter x1, waiting for transfers between devices, body(): lax.psum_scatter(partial_out.astype(jnp.bfloat16), 'tp', scatter_dimensio...  19.7 us
    psum x1, waiting for transfers between devices, unit_totals(): return lax.psum(paired.astype(jnp.bfloat16), 'tp').astype(jnp.float32)  13.5 us
    all_gather x1, blocking collectives, body(): lax.all_gather(lax.all_to_all(outgoing, 'ep', split_axis=0, concat_axis=0...  9.93 us
    psum x1, blocking collectives, body(): lax.psum((jnp.sum(middle_own * middle_own, axis=-1), jnp.sum(middle_own *...  5.76 us
  transfers between devices with their start and end apart: 6, of which 6 were waited for; matrix products, arithmetic and copies ran while one was open for 11% of the time, Pallas kernels for 0%

commit v1 on v0

--- a/solution.py
+++ b/solution.py
@@ -20,7 +20,7 @@
 
 
 def unit_totals(paired):
-    return lax.psum(paired.astype(jnp.bfloat16), "tp").astype(jnp.float32)
+    return jnp.sum(lax.all_gather(paired.astype(jnp.bfloat16), "tp"), axis=0).astype(jnp.float32)
 
 
 def body(

time: 233 us -> 220 us (0.944)
  waiting for transfers between devices: 109 us -> 90.1 us
  blocking collectives: 47.2 us -> 60.4 us
  starting transfers between devices: 11 us -> 5.68 us
    psum x1 -> x0, waiting for transfers between devices: 13.5 us -> none  [unit_totals(): return lax.psum(paired.astype(jnp.bfloat16), 'tp').astype(jnp.float32)]
    all_to_all x0 -> x1, blocking collectives: none -> 12.5 us  [body(): lax.all_to_all(outgoing, 'ep', split_axis=0, concat_axis=0, tiled=True)]
    reduce_scatter x1, waiting for transfers between devices: 20 us -> 14.7 us  [body(): lax.psum_scatter(block_out.astype(jnp.bfloat16), 'tp', scatter_dimension=...]
    all_to_all x1 -> x0, starting transfers between devices: 5.32 us -> none  [body(): lax.all_to_all(outgoing, 'ep', split_axis=0, concat_axis=0, tiled=True)]
    reduce_sum x0 -> x1, other arithmetic: none -> 3.63 us  [unit_totals(): jnp.sum(lax.all_gather(paired.astype(jnp.bfloat16), 'tp'), axis=0)]
    all_to_all x1 -> x0, waiting for transfers between devices: 3.48 us -> none  [body(): lax.all_to_all(outgoing, 'ep', split_axis=0, concat_axis=0, tiled=True)]
  transfers between devices with their start and end apart: 6 -> 5, of which waited for: 6 -> 4; matrix products, arithmetic and copies ran while one was open for 11% -> 11% of each run, Pallas kernels for 0% -> 0%
where the time goes in v1:
time: 220 us
  waiting for transfers between devices  90.1 us (41%)
  blocking collectives  60.4 us (27%)
  matrix products  23.9 us (11%)
  other arithmetic  17.5 us (8%)
  between operations  14 us (6%)
  local copies, waits for them, and re-layouts  7.78 us (4%)
  starting transfers between devices  5.68 us (3%)
    reduce_scatter x1, waiting for transfers between devices, body(): lax.psum_scatter(matmul(dense_hidden, dense_down).astype(jnp.bfloat16), '...  47.1 us
    all_gather x1, blocking collectives, body(): piece = lax.all_gather(ffn_own, 'ep', axis=0, tiled=True)  31.5 us
    reduce_scatter x1, waiting for transfers between devices, body(): lax.psum_scatter(partial_out.astype(jnp.bfloat16), 'tp', scatter_dimensio...  21 us
    dot_general x11, matrix products, matmul(): return jnp.dot(left, right, preferred_element_type=jnp.float32)  20.8 us
    reduce_scatter x1, waiting for transfers between devices, body(): lax.psum_scatter(block_out.astype(jnp.bfloat16), 'tp', scatter_dimension=...  14.7 us
    all_to_all x1, blocking collectives, body(): lax.all_to_all(outgoing, 'ep', split_axis=0, concat_axis=0, tiled=True)  12.5 us
    all_gather x1, blocking collectives, body(): lax.all_gather(lax.all_to_all(outgoing, 'ep', split_axis=0, concat_axis=0...  10.7 us
    all_to_all x1, waiting for transfers between devices, body(): lax.all_to_all(summed.reshape(sources, items, quarter).astype(jnp.bfloat1...  7.23 us
  transfers between devices with their start and end apart: 5, of which 4 were waited for; matrix products, arithmetic and copies ran while one was open for 11% of the time, Pallas kernels for 0%

profile of v1, /device:TPU:0, one launch (start us, length us, event | category | flops | bytes accessed | tf_op | source)
XLA Modules:
  0.0 219.5 jit_solution(2537083607108326177)
XLA Ops:
  7.2 0.0 copy-start
  7.2 0.0 reduce-scatter.4.cloned.1.call-start
  7.2 0.8 convert_element_type.113
  8.1 1.1 multiply_reduce_fusion
  9.2 1.7 fusion.20
  10.9 1.4 fusion.21
  12.3 1.4 fusion.23
  13.7 1.4 fusion.52
  15.1 4.5 %multiply_add_fusion = f32[48,1,128,256]{3,2,1,0:T(8,128)S(1)} fusion(f32[48,1,128,256]{3,2,1,0:T(8,128)} %param.22, f32[48,256]{1,0:T(8,128)S(1)} %fusion.20, f32[48,128]{1,0:T(8,128)S(1)} %fusion.21, f32[48,128]{1,0:T(8,128)S(1)} %fusion.52), kind=kLoop, calls=%fused_computation.3 | loop fusion | flops 4718592 | bytes 12681216 | tf_op jit(solution)/shard_map/add | solution.py:66
  19.6 0.0 copy-start.1
  19.6 3.1 %fusion = f32[48,1,256]{2,1,0:T(1,128)S(1)} fusion(f32[48,128,1]{1,2,0:T(1,128)S(1)} %bitcast.59, f32[48,1,128,256]{3,2,1,0:T(8,128)S(1)} %multiply_add_fusion), kind=kOutput, calls=%fused_computation.1 | convolution fusion | flops 18874368 | bytes 6365184 | tf_op jit(solution)/shard_map/bhk,bhkv->bhv/dot_general | solution.py:67
  22.7 0.1 fusion.41
  22.9 3.0 %convolution_convert_fusion = bf16[48,2048]{1,0:T(8,128)(2,1)} fusion(bf16[256,2048]{1,0:T(8,128)(2,1)} %param.31, bf16[2048,256]{1,0:T(8,128)(2,1)} %param.27, f32[48,1,256]{2,1,0:T(1,128)S(1)} %fusion, f32[256]{0:T(256)S(1)} %bitcast.60, f32[48]{0:T(128)S(1)} %add_rsqrt_fusion.1, f32[2048]{0:T(1024)S(1)} %convert_element_type.113, ...), kind=kOutput, calls=%fused_computation.11 | convolution fusion | flops 101277696 | bytes 2549120 | tf_op jit(solution)/shard_map/dot_general | solution.py:19
  25.9 0.0 reduce-scatter.4.cloned.1.call-update
  25.9 0.0 all-gather.2.cloned.1.call-start
  26.0 0.0 copy-start.3
  26.0 0.8 convert_element_type.112
  26.8 0.8 dynamic-slice_convert_fusion
  27.5 21.0 %reduce-scatter.4.cloned.1.call-done = bf16[48,512]{1,0:T(8,128)(2,1)} async-done(((bf16[48,2048]{1,0:T(8,128)(2,1)}), bf16[48,512]{1,0:T(8,128)(2,1)}) %reduce-scatter.4.cloned.1.call-update) | async-done | bytes 49168 | tf_op jit(solution)/shard_map/reduce_scatter | solution.py:75
  48.6 0.9 add_convert_fusion
  49.5 0.1 fusion.35
  49.6 5.8 %all-reduce = (f32[48]{0:T(128)S(1)}, f32[48]{0:T(128)S(1)}) all-reduce(f32[48]{0:T(128)S(1)} %get-tuple-element.3, f32[48]{0:T(128)S(1)} %get-tuple-element.2), channel_id=1, replica_groups=mesh['ep'=8,'tp'=4] {'tp'}, use_global_device_ids=true, to_apply=%region_6.7 | all-reduce | flops 96 | bytes 768 | tf_op jit(solution)/shard_map/psum | solution.py:79
  55.4 0.1 fusion.38
  55.5 31.5 %all_gather.10 = bf16[384,512]{1,0:T(8,128)(2,1)S(1)} all-gather(bf16[48,512]{1,0:T(8,128)(2,1)S(1)} %fusion.38), channel_id=1, replica_groups=mesh['ep'=8,'tp'=4] {'ep'}, dimensions={0}, use_global_device_ids=true | all-gather | bytes 442368 | tf_op jit(solution)/shard_map/all_gather | solution.py:133
  87.0 1.4 fusion.11
  88.5 1.4 fusion.12
  89.9 1.0 pad_maximum_fusion
  90.9 0.0 all-gather.2.cloned.1.call-update
  90.9 0.0 reduce-scatter.8.cloned.1.call-start
  90.9 0.1 copy.40
  91.0 0.1 eq.29
  91.2 0.1 fusion.45
  91.3 0.1 reduce_window_sum.11
  91.4 0.2 select_reduce_fusion
  91.6 0.1 reshape.166
  91.7 0.1 copy.41
  91.8 0.1 fusion.48
  91.9 0.2 convolution_convert_fusion.4
  92.1 12.5 %all_to_all.10 = bf16[8,14,512]{2,1,0:T(8,128)(2,1)S(1)} all-to-all(bf16[8,14,512]{2,1,0:T(8,128)(2,1)S(1)} %reshape.167), channel_id=1, replica_groups=mesh['ep'=8,'tp'=4] {'ep'}, dimensions={0} | all-to-all | bytes 229376 | tf_op jit(solution)/shard_map/all_to_all | solution.py:108
  104.6 10.7 %all_gather.12 = bf16[8,14,2048]{2,1,0:T(8,128)(2,1)} all-gather(bf16[8,14,512]{2,1,0:T(8,128)(2,1)S(1)} %all_to_all.10), channel_id=1, replica_groups=mesh['ep'=8,'tp'=4] {'tp'}, dimensions={2}, use_global_device_ids=true | all-gather | bytes 573440 | tf_op jit(solution)/shard_map/all_gather | solution.py:107
  115.3 2.0 reshape.168
  117.2 2.6 %fusion.6 = f32[112,768]{1,0:T(8,128)S(1)} fusion(bf16[112,2048]{1,0:T(8,128)(2,1)} %reshape.168, bf16[1,2048,768]{2,1,0:T(8,128)(2,1)} %param.36), kind=kOutput, calls=%fused_computation.8 | convolution fusion | flops 352321536 | bytes 3948544 | tf_op jit(solution)/shard_map/dot_general | solution.py:19
  119.9 4.1 %fusion.8 = bf16[112,2048]{1,0:T(8,128)(2,1)} fusion(bf16[1,768,2048]{2,1,0:T(8,128)(2,1)S(1)} %copy-done, bf16[112,2048]{1,0:T(8,128)(2,1)} %reshape.168, bf16[1,2048,768]{2,1,0:T(8,128)(2,1)} %param.37, f32[112,768]{1,0:T(8,128)S(1)} %fusion.6), kind=kOutput, calls=%fused_computation.10 | convolution fusion | flops 705388544 | bytes 7553024 | tf_op jit(solution)/shard_map/dot_general | solution.py:19
  124.0 0.0 reduce-scatter.8.cloned.1.call-update
  124.0 0.0 reduce-scatter.6.cloned.1.call-start
  124.0 0.0 all-gather.2.cloned.1.call-done
  124.1 3.6 %reduce_sum.82 = bf16[384,1024]{1,0:T(8,128)(2,1)} reduce(bf16[4,384,1024]{2,1,0:T(8,128)(2,1)} %all-gather.2.cloned.1.call-done, bf16[]{:T(256)} %constant.59.clone.1), dimensions={0}, to_apply=%region_7.8 | reduce | flops 1179648 | bytes 3932162 | tf_op jit(solution)/shard_map/reduce_sum | solution.py:23
  127.7 1.3 convert_element_type.131
  129.0 2.2 convolution_convert_fusion.1
  131.2 0.0 reduce-scatter.6.cloned.1.call-update
  131.2 0.1 copy.43
  131.3 0.1 reshape.171
  131.4 14.7 %reduce-scatter.8.cloned.1.call-done = bf16[112,512]{1,0:T(8,128)(2,1)} async-done(((bf16[112,2048]{1,0:T(8,128)(2,1)}), bf16[112,512]{1,0:T(8,128)(2,1)}) %reduce-scatter.8.cloned.1.call-update) | async-done | bytes 114704 | tf_op jit(solution)/shard_map/reduce_scatter | solution.py:120
  146.1 1.6 convert_element_type.140
  147.7 5.5 %all-to-all-start.1 = ((bf16[8,14,512]{2,1,0:T(8,128)(2,1)}), bf16[8,14,512]{2,1,0:T(8,128)(2,1)}, u32[]{:S(2)}, u32[]{:S(2)}) async-start(bf16[8,14,512]{2,1,0:T(8,128)(2,1)} %convert_element_type.140), calls=%async_computation.4 | async-start | bytes 262144 | tf_op jit(solution)/shard_map/all_to_all | solution.py:123
  153.2 0.1 copy.42
  153.3 0.1 copy.44
  153.4 7.2 %all-to-all-done.1 = bf16[8,14,512]{2,1,0:T(8,128)(2,1)} async-done(((bf16[8,14,512]{2,1,0:T(8,128)(2,1)}), bf16[8,14,512]{2,1,0:T(8,128)(2,1)}, u32[]{:S(2)}, u32[]{:S(2)}) %all-to-all-start.1) | async-done | bytes 114720 | tf_op jit(solution)/shard_map/all_to_all | solution.py:123
  160.7 0.9 reshape.174
  161.6 1.4 gather_fusion
  163.0 1.0 gather.7
  164.0 0.3 multiply_reduce_fusion.1
  164.4 47.1 %reduce-scatter.6.cloned.1.call-done = bf16[48,512]{1,0:T(8,128)(2,1)} async-done(((bf16[384,512]{1,0:T(8,128)(2,1)}), bf16[48,512]{1,0:T(8,128)(2,1)}) %reduce-scatter.6.cloned.1.call-update) | async-done | bytes 49168 | tf_op jit(solution)/shard_map/reduce_scatter | solution.py:139
  211.5 1.5 fusion.40
  (17 shorter events, 0.1 us)
Async XLA Ops:
  7.2 112.7 %copy-start = (bf16[1,768,2048]{2,1,0:T(8,128)(2,1)S(1)}, bf16[1,768,2048]{2,1,0:T(8,128)(2,1)}, u32[]{:S(2)}) copy-start(bf16[1,768,2048]{2,1,0:T(8,128)(2,1)} %param.38) | copy-start | bytes 9437188
  7.2 41.4 %reduce-scatter.4.cloned.1.call-start = ((), (), s32[]{:S(2)}) async-start(), calls=%async_computation.5 | async-start | bytes 245760 | tf_op jit(solution)/shard_map/reduce_scatter | solution.py:75
  19.6 3.1 %copy-start.1 = (f32[48,1,128,256]{3,2,1,0:T(8,128)}, f32[48,1,128,256]{3,2,1,0:T(8,128)S(1)}, u32[]{:S(2)}) copy-start(f32[48,1,128,256]{3,2,1,0:T(8,128)S(1)} %multiply_add_fusion) | copy-start | bytes 18874372
  19.6 3.2 %copy-start.5 = (bf16[1,256]{1,0:T(2,128)(2,1)S(1)}, bf16[1,256]{1,0:T(2,128)(2,1)}, u32[]{:S(2)}) copy-start(bf16[1,256]{1,0:T(2,128)(2,1)} %param.30) | copy-start | bytes 1540
  19.6 3.3 %copy-start.2 = (bf16[48,2048]{1,0:T(8,128)(2,1)S(1)}, bf16[48,2048]{1,0:T(8,128)(2,1)}, u32[]{:S(2)}) copy-start(bf16[48,2048]{1,0:T(8,128)(2,1)} %param.21) | copy-start | bytes 589828
  25.9 98.1 %all-gather.2.cloned.1.call-start = ((), (), s32[]{:S(2)}) async-start(), calls=%async_computation.6 | async-start | bytes 3932160 | tf_op jit(solution)/shard_map/all_gather | solution.py:23
  26.0 65.0 %copy-start.3 = (s32[48,2]{0,1:T(2,128)S(1)}, s32[48,2]{0,1:T(2,128)}, u32[]{:S(2)}) copy-start(s32[48,2]{0,1:T(2,128)} %param.34) | copy-start | bytes 1156
  90.9 55.2 %reduce-scatter.8.cloned.1.call-start = ((), (), s32[]{:S(2)}) async-start(), calls=%async_computation.8 | async-start | bytes 573440 | tf_op jit(solution)/shard_map/reduce_scatter | solution.py:120
  124.0 87.5 %reduce-scatter.6.cloned.1.call-start = ((), (), s32[]{:S(2)}) async-start(), calls=%async_computation.7 | async-start | bytes 442368 | tf_op jit(solution)/shard_map/reduce_scatter | solution.py:139
  129.0 24.3 %copy-start.4 = (f32[48,2]{0,1:T(2,128)S(1)}, f32[48,2]{0,1:T(2,128)}, u32[]{:S(2)}) copy-start(f32[48,2]{0,1:T(2,128)} %param.35) | copy-start | bytes 1156
  147.7 13.0 %all-to-all-start.1 = ((bf16[8,14,512]{2,1,0:T(8,128)(2,1)}), bf16[8,14,512]{2,1,0:T(8,128)(2,1)}, u32[]{:S(2)}, u32[]{:S(2)}) async-start(bf16[8,14,512]{2,1,0:T(8,128)(2,1)} %convert_element_type.140), calls=%async_computation.4 | async-start | bytes 262144 | tf_op jit(solution)/shard_map/all_to_all | solution.py:123
Sparse Core Ops, SparseCore 0:
  26.1 22.4 reduce-scatter.3
  91.0 31.2 all-gather.1
  124.8 21.2 reduce-scatter.7
  149.2 62.2 reduce-scatter.5
